TPU v7x, 32 devices: a whole 2x2x4 slice. The times are simulated.
32 devices in a mesh: fs: 4 (over z), rep: 4 (over y, x), tp: 2 (over core).
Axes of the slice: x: 2, y: 2, z: 4, core: 2. Of those that a mesh axis runs over, the one named last changes fastest.
Arguments:
- normed_input: bfloat16 [2048, 1024], P(('fs', 'rep')), may hold values from -6 to 6
- query_cotangent: bfloat16 [2048, 512], P(('fs', 'rep'), 'tp'), may hold values from -0.029907227 to 0.029907227
- value_cotangent: bfloat16 [2048, 1024], P(('fs', 'rep'), 'tp'), may hold values from -0.029907227 to 0.029907227
- query_basis: bfloat16 [1024, 128], replicated, may hold values from -0.1875 to 0.1875
- value_basis: bfloat16 [1024, 128], replicated, may hold values from -0.1875 to 0.1875
- query_weight: float32 [1024, 512], P(('fs', 'rep'), 'tp'), may hold values from -0.1875 to 0.1875
- value_weight: float32 [1024, 1024], P(('fs', 'rep'), 'tp'), may hold values from -0.1875 to 0.1875
- query_first: float32 [128, 512], P(('fs', 'rep'), 'tp'), may hold values from -6 to 6
- query_second: float32 [128, 512], P(('fs', 'rep'), 'tp'), may hold values from 0.25 to 4
- value_first: float32 [128, 1024], P(('fs', 'rep'), 'tp'), may hold values from -6 to 6
- value_second: float32 [128, 1024], P(('fs', 'rep'), 'tp'), may hold values from 0.25 to 4
Outputs:
- query_update: float32 [1024, 512], P(('fs', 'rep'), 'tp')
- value_update: float32 [1024, 1024], P(('fs', 'rep'), 'tp')
- query_weight_new: float32 [1024, 512], P(('fs', 'rep'), 'tp')
- value_weight_new: float32 [1024, 1024], P(('fs', 'rep'), 'tp')
- query_first_new: float32 [128, 512], P(('fs', 'rep'), 'tp')
- query_second_new: float32 [128, 512], P(('fs', 'rep'), 'tp')
- value_first_new: float32 [128, 1024], P(('fs', 'rep'), 'tp')
- value_second_new: float32 [128, 1024], P(('fs', 'rep'), 'tp')
- query_copy: bfloat16 [1024, 512], P(None, 'tp')
- value_copy: bfloat16 [1024, 1024], P(None, 'tp')
All inputs are finite; a program needn't handle non-finite values.
Results may differ from a plain program's by a relative error of at most 0.001.
Values may be sent and summed in bfloat16 or wider, within the bound.
A program may use at most 64 MiB of HBM per device.

v0:
```python
import jax
import jax.numpy as jnp
from jax import lax
from jax.sharding import PartitionSpec as P


def moments(projected, first_old, second_old):
    first_new = 0.9 * first_old + 0.1 * projected
    second_new = 0.99 * second_old + 0.01 * projected * projected
    return (first_new, second_new, first_new / (jnp.sqrt(second_new) + 1e-08))


def finish(whole_dir, basis_rows, weight, squares, entries):
    norm_scale = jnp.sqrt(squares / entries + 1.0)
    update = jnp.dot(basis_rows, whole_dir, precision=lax.Precision.HIGHEST) / norm_scale
    weight_new = weight - 0.01 * update
    return (update, weight_new, weight_new.astype(jnp.bfloat16))


def split_parts(reduced):
    high_part = reduced.astype(jnp.bfloat16)
    held = lax.optimization_barrier(high_part)
    low_part = (reduced - held.astype(jnp.float32)).astype(jnp.bfloat16)
    return (high_part, low_part)


def parts_product(high_part, low_part, cotangent):
    dims = (((0,), (0,)), ((), ()))
    first_term = lax.dot_general(high_part, cotangent, dims, preferred_element_type=jnp.float32)
    second_term = lax.dot_general(low_part, cotangent, dims, preferred_element_type=jnp.float32)
    return first_term + second_term


def body(
    normed_input,
    query_cotangent,
    value_cotangent,
    query_basis,
    value_basis,
    query_weight,
    value_weight,
    query_first,
    query_second,
    value_first,
    value_second,
):
    row_count = query_weight.shape[0]
    query_width = query_cotangent.shape[1]
    offset = lax.axis_index(("fs", "rep")) * row_count
    query_rows = lax.dynamic_slice_in_dim(query_basis, offset, row_count, 0).astype(jnp.float32)
    value_rows = lax.dynamic_slice_in_dim(value_basis, offset, row_count, 0).astype(jnp.float32)
    reduced_query = jnp.dot(normed_input, query_basis, preferred_element_type=jnp.float32)
    reduced_value = jnp.dot(normed_input, value_basis, preferred_element_type=jnp.float32)
    query_high, query_low = split_parts(reduced_query)
    value_high, value_low = split_parts(reduced_value)
    projected = lax.psum_scatter(
        jnp.concatenate(
            [
                parts_product(query_high, query_low, query_cotangent),
                parts_product(value_high, value_low, value_cotangent),
            ],
            axis=1,
        ),
        ("fs", "rep"),
        scatter_dimension=0,
        tiled=True,
    )
    query_projected = projected[:, :query_width]
    value_projected = projected[:, query_width:]
    query_first_new, query_second_new, query_dir = moments(
        query_projected, query_first, query_second
    )
    value_first_new, value_second_new, value_dir = moments(
        value_projected, value_first, value_second
    )
    query_whole, value_whole = (
        lax.all_gather(query_dir, ("fs", "rep"), axis=0, tiled=True),
        lax.all_gather(value_dir, ("fs", "rep"), axis=0, tiled=True),
    )
    query_squares, value_squares = lax.psum(
        (jnp.sum(query_dir * query_dir), jnp.sum(value_dir * value_dir)), ("fs", "rep", "tp")
    )
    tp_count = lax.axis_size("tp")
    query_update, query_weight_new, query_half = finish(
        query_whole,
        query_rows,
        query_weight,
        query_squares,
        query_whole.shape[0] * query_whole.shape[1] * tp_count,
    )
    value_update, value_weight_new, value_half = finish(
        value_whole,
        value_rows,
        value_weight,
        value_squares,
        value_whole.shape[0] * value_whole.shape[1] * tp_count,
    )
    query_copy, value_copy = (
        lax.all_gather(query_half, ("fs", "rep"), axis=0, tiled=True),
        lax.all_gather(value_half, ("fs", "rep"), axis=0, tiled=True),
    )
    return (
        query_update,
        value_update,
        query_weight_new,
        value_weight_new,
        query_first_new,
        query_second_new,
        value_first_new,
        value_second_new,
        query_copy,
        value_copy,
    )


def solution(mesh):
    in_specs = (
        P(("fs", "rep"), None),
        P(("fs", "rep"), "tp"),
        P(("fs", "rep"), "tp"),
        P(),
        P(),
        P(("fs", "rep"), "tp"),
        P(("fs", "rep"), "tp"),
        P(("fs", "rep"), "tp"),
        P(("fs", "rep"), "tp"),
        P(("fs", "rep"), "tp"),
        P(("fs", "rep"), "tp"),
    )
    out_specs = (
        P(("fs", "rep"), "tp"),
        P(("fs", "rep"), "tp"),
        P(("fs", "rep"), "tp"),
        P(("fs", "rep"), "tp"),
        P(("fs", "rep"), "tp"),
        P(("fs", "rep"), "tp"),
        P(("fs", "rep"), "tp"),
        P(("fs", "rep"), "tp"),
        P(None, "tp"),
        P(None, "tp"),
    )
    return jax.shard_map(body, mesh=mesh, in_specs=in_specs, out_specs=out_specs, check_vma=False)
```

profile of v0, /device:TPU:0, one launch (start us, length us, event | category | flops | bytes accessed | tf_op | source)
XLA Modules:
  0.0 313.8 jit_solution(15066968954675229272)
XLA Ops:
  7.2 0.0 reduce-scatter.2.cloned.1.call-start
  7.2 0.9 copy-done
  8.1 1.2 fusion.10
  9.4 0.2 fusion.13
  9.6 0.7 copy-done.2
  10.3 0.2 fusion.11
  10.5 0.6 copy-done.5
  11.1 0.2 fusion.12
  11.3 0.2 convolution_add_fusion
  11.6 0.2 convolution_add_fusion.1
  11.8 0.8 pad_maximum_fusion
  12.6 0.0 all-gather.2.cloned.1.call-start
  12.7 126.3 %reduce-scatter.2.cloned.1.call-done = f32[8,768]{1,0:T(8,128)} async-done(((f32[128,768]{1,0:T(8,128)}), f32[8,768]{1,0:T(8,128)}) %reduce-scatter.2.cloned.1.call-update) | async-done | bytes 24592 | tf_op jit(solution)/shard_map/reduce_scatter | solution.py:56
  138.9 1.9 multiply_reduce_fusion
  140.9 1.9 multiply_reduce_fusion.1
  142.8 40.4 %all-reduce = (f32[]{:T(128)}, f32[]{:T(128)}) all-reduce(f32[]{:T(128)} %get-tuple-element.20, f32[]{:T(128)} %get-tuple-element.16), channel_id=1, replica_groups=mesh['fs'=4,'rep'=4,'tp'=2] {'fs','rep','tp'}, use_global_device_ids=true, to_apply=%region_2.0 | all-reduce | flops 2 | bytes 16 | tf_op jit(solution)/shard_map/psum | solution.py:80
  183.9 40.3 %all_gather.13 = f32[128,512]{1,0:T(8,128)S(1)} all-gather(f32[8,512]{1,0:T(8,128)S(1)} %get-tuple-element.17), channel_id=1, replica_groups=mesh['fs'=4,'rep'=4,'tp'=2] {'fs','rep'}, dimensions={0}, use_global_device_ids=true | all-gather | bytes 278528 | tf_op jit(solution)/shard_map/all_gather | solution.py:78
  224.2 1.0 fusion.6
  225.9 36.5 %all_gather.12 = f32[128,256]{1,0:T(8,128)S(1)} all-gather(f32[8,256]{1,0:T(8,128)S(1)} %get-tuple-element.21), channel_id=1, replica_groups=mesh['fs'=4,'rep'=4,'tp'=2] {'fs','rep'}, dimensions={0}, use_global_device_ids=true | all-gather | bytes 139264 | tf_op jit(solution)/shard_map/all_gather | solution.py:77
  262.3 0.8 fusion.7
  263.2 41.4 %all_gather.14 = bf16[1024,256]{1,0:T(8,128)(2,1)S(1)} all-gather(bf16[64,256]{1,0:T(8,128)(2,1)S(1)} %get-tuple-element.14), channel_id=1, replica_groups=mesh['fs'=4,'rep'=4,'tp'=2] {'fs','rep'}, dimensions={0}, use_global_device_ids=true | all-gather | bytes 557056 | tf_op jit(solution)/shard_map/all_gather | solution.py:99
  304.5 0.8 copy.23
  305.3 0.6 copy-done.1
  306.0 1.0 copy.24
  (23 shorter events, 0.1 us)
Async XLA Ops:
  7.2 1.0 copy-start
  7.2 2.2 copy-start.3
  7.2 131.7 %reduce-scatter.2.cloned.1.call-start = ((), (), s32[]{:S(2)}) async-start(), calls=%async_computation.1 | async-start | bytes 417792 | tf_op jit(solution)/shard_map/reduce_scatter | solution.py:56
  8.1 1.5 copy-start.4
  9.3 1.0 copy-start.2
  10.3 0.8 copy-start.5
  12.5 126.4 %copy-start.9 = (f32[8,512]{1,0:T(8,128)S(1)}, f32[8,512]{1,0:T(8,128)}, u32[]{:S(2)}) copy-start(f32[8,512]{1,0:T(8,128)} %param.20) | copy-start | bytes 49156
  12.6 126.4 %copy-start.8 = (f32[8,512]{1,0:T(8,128)S(1)}, f32[8,512]{1,0:T(8,128)}, u32[]{:S(2)}) copy-start(f32[8,512]{1,0:T(8,128)} %param.21) | copy-start | bytes 49156
  12.6 292.0 %all-gather.2.cloned.1.call-start = ((), (), s32[]{:S(2)}) async-start(), calls=%async_computation.2 | async-start | bytes 1114112 | tf_op jit(solution)/shard_map/all_gather | solution.py:100
  12.6 128.2 %copy-start.10 = (f32[8,256]{1,0:T(8,128)S(1)}, f32[8,256]{1,0:T(8,128)}, u32[]{:S(2)}) copy-start(f32[8,256]{1,0:T(8,128)} %param.19) | copy-start | bytes 24580
  12.6 128.2 %copy-start.11 = (f32[8,256]{1,0:T(8,128)S(1)}, f32[8,256]{1,0:T(8,128)}, u32[]{:S(2)}) copy-start(f32[8,256]{1,0:T(8,128)} %param.18) | copy-start | bytes 24580
  183.9 40.3 %copy-start.6 = (f32[64,512]{1,0:T(8,128)S(1)}, f32[64,512]{1,0:T(8,128)}, u32[]{:S(2)}) copy-start(f32[64,512]{1,0:T(8,128)} %param.17) | copy-start | bytes 393220
  225.9 36.5 %copy-start.7 = (f32[64,256]{1,0:T(8,128)S(1)}, f32[64,256]{1,0:T(8,128)}, u32[]{:S(2)}) copy-start(f32[64,256]{1,0:T(8,128)} %param.16) | copy-start | bytes 196612
  304.5 1.4 copy-start.1
Sparse Core Ops, SparseCore 0:
  13.2 125.6 reduce-scatter.1
  225.3 52.1 all-gather.1
where the time goes:
time: 314 us
  blocking collectives  159 us (51%)
  waiting for transfers between devices  126 us (40%)
  between operations  15.6 us (5%)
  local copies, waits for them, and re-layouts  4.65 us (1%)
  other arithmetic  4.61 us (1%)
  matrix products  4.03 us (1%)
    reduce_scatter x1, waiting for transfers between devices, body(): lax.psum_scatter(jnp.concatenate([parts_product(query_high, query_low, qu...  126 us
    all_gather x1, blocking collectives, body(): lax.all_gather(query_half, ('fs', 'rep'), axis=0, tiled=True)  41.4 us
    psum x1, blocking collectives, body(): lax.psum((jnp.sum(query_dir * query_dir), jnp.sum(value_dir * value_dir))...  40.4 us
    all_gather x1, blocking collectives, body(): lax.all_gather(value_dir, ('fs', 'rep'), axis=0, tiled=True)  40.3 us
    all_gather x1, blocking collectives, body(): lax.all_gather(query_dir, ('fs', 'rep'), axis=0, tiled=True)  36.5 us
  transfers between devices with their start and end apart: 2, of which 1 were waited for; matrix products, arithmetic and copies ran while one was open for 0% of the time, Pallas kernels for 0%

commit v1 on v0

--- a/solution.py
+++ b/solution.py
@@ -2,6 +2,7 @@
 import jax.numpy as jnp
 from jax import lax
 from jax.sharding import PartitionSpec as P
+from jax.lax import all_to_all, axis_size
 
 
 def moments(projected, first_old, second_old):
@@ -44,6 +45,18 @@
     value_first,
     value_second,
 ):
+
+    def settle_slices_on(mine, mesh_dim, array_axis):
+        return jnp.concatenate(
+            all_to_all(
+                jnp.stack([mine for _ in range(axis_size(mesh_dim))]),
+                concat_axis=0,
+                axis_name=mesh_dim,
+                split_axis=0,
+            ),
+            axis=array_axis,
+        )
+
     row_count = query_weight.shape[0]
     query_width = query_cotangent.shape[1]
     offset = lax.axis_index(("fs", "rep")) * row_count
@@ -74,7 +87,7 @@
         value_projected, value_first, value_second
     )
     query_whole, value_whole = (
-        lax.all_gather(query_dir, ("fs", "rep"), axis=0, tiled=True),
+        settle_slices_on(query_dir, ("fs", "rep"), 0),
         lax.all_gather(value_dir, ("fs", "rep"), axis=0, tiled=True),
     )
     query_squares, value_squares = lax.psum(

time: 314 us -> 289 us (0.920)
  blocking collectives: 159 us -> 122 us
  waiting for transfers between devices: 126 us -> 134 us
  starting transfers between devices: 0.08 us -> 3.72 us
    all_gather x1 -> x0, blocking collectives: 36.5 us -> none  [body(): lax.all_gather(query_dir, ('fs', 'rep'), axis=0, tiled=True)]
    all_to_all x0 -> x1, waiting for transfers between devices: none -> 7.27 us  [settle_slices_on(): all_to_all(jnp.stack([mine for _ in range(axis_size(mesh_dim))]), concat_...]
    all_to_all x0 -> x1, starting transfers between devices: none -> 3.64 us  [settle_slices_on(): all_to_all(jnp.stack([mine for _ in range(axis_size(mesh_dim))]), concat_...]
  transfers between devices with their start and end apart: 2 -> 3, of which waited for: 1 -> 2; matrix products, arithmetic and copies ran while one was open for 0% -> 1% of each run, Pallas kernels for 0% -> 0%
where the time goes in v1:
time: 289 us
  waiting for transfers between devices  134 us (46%)
  blocking collectives  122 us (42%)
  between operations  15.6 us (5%)
  local copies, waits for them, and re-layouts  5.31 us (2%)
  other arithmetic  4.61 us (2%)
  matrix products  4.03 us (1%)
  starting transfers between devices  3.72 us (1%)
    reduce_scatter x1, waiting for transfers between devices, body(): lax.psum_scatter(jnp.concatenate([parts_product(query_high, query_low, qu...  126 us
    all_gather x1, blocking collectives, body(): lax.all_gather(query_half, ('fs', 'rep'), axis=0, tiled=True)  41.1 us
    psum x1, blocking collectives, body(): lax.psum((jnp.sum(query_dir * query_dir), jnp.sum(value_dir * value_dir))...  40.4 us
    all_gather x1, blocking collectives, body(): lax.all_gather(value_dir, ('fs', 'rep'), axis=0, tiled=True)  40.3 us
    all_to_all x1, waiting for transfers between devices, settle_slices_on(): all_to_all(jnp.stack([mine for _ in range(axis_size(mesh_dim))]), concat_...  7.27 us
  transfers between devices with their start and end apart: 3, of which 2 were waited for; matrix products, arithmetic and copies ran while one was open for 1% of the time, Pallas kernels for 0%

profile of v1, /device:TPU:0, one launch (start us, length us, event | category | flops | bytes accessed | tf_op | source)
XLA Modules:
  0.0 288.6 jit_solution(9641706617914831413)
XLA Ops:
  7.2 0.9 copy-done
  8.1 1.2 fusion.11
  9.4 0.2 fusion.14
  9.6 0.7 copy-done.2
  10.3 0.2 fusion.12
  10.5 0.6 copy-done.5
  11.1 0.2 fusion.13
  11.3 0.2 convolution_add_fusion
  11.6 0.2 convolution_add_fusion.1
  11.8 0.8 pad_maximum_fusion
  12.7 126.3 %reduce-scatter.2.cloned.1.call-done = f32[8,768]{1,0:T(8,128)} async-done(((f32[128,768]{1,0:T(8,128)}), f32[8,768]{1,0:T(8,128)}) %reduce-scatter.2.cloned.1.call-update) | async-done | bytes 24592 | tf_op jit(solution)/shard_map/reduce_scatter | solution.py:69
  138.9 1.9 multiply_reduce_fusion
  140.9 1.9 multiply_reduce_fusion.1
  142.8 40.4 %all-reduce = (f32[]{:T(128)}, f32[]{:T(128)}) all-reduce(f32[]{:T(128)} %get-tuple-element.20, f32[]{:T(128)} %get-tuple-element.16), channel_id=1, replica_groups=mesh['fs'=4,'rep'=4,'tp'=2] {'fs','rep','tp'}, use_global_device_ids=true, to_apply=%region_2.0 | all-reduce | flops 2 | bytes 16 | tf_op jit(solution)/shard_map/psum | solution.py:93
  183.9 40.3 %all_gather.9 = f32[128,512]{1,0:T(8,128)S(1)} all-gather(f32[8,512]{1,0:T(8,128)S(1)} %get-tuple-element.17), channel_id=1, replica_groups=mesh['fs'=4,'rep'=4,'tp'=2] {'fs','rep'}, dimensions={0}, use_global_device_ids=true | all-gather | bytes 278528 | tf_op jit(solution)/shard_map/all_gather | solution.py:91
  224.2 1.0 fusion.7
  225.2 0.7 stack.2
  225.9 3.6 %all-to-all-start = ((f32[16,8,256]{2,1,0:T(8,128)}), f32[16,8,256]{2,1,0:T(8,128)S(1)}, u32[]{:S(2)}, u32[]{:S(2)}) async-start(f32[16,8,256]{2,1,0:T(8,128)} %stack.2), calls=%async_computation.1 | async-start | bytes 262144 | tf_op jit(solution)/shard_map/all_to_all | solution.py:51
  230.2 7.3 %all-to-all-done = f32[16,8,256]{2,1,0:T(8,128)S(1)} async-done(((f32[16,8,256]{2,1,0:T(8,128)}), f32[16,8,256]{2,1,0:T(8,128)S(1)}, u32[]{:S(2)}, u32[]{:S(2)}) %all-to-all-start) | async-done | bytes 131104 | tf_op jit(solution)/shard_map/all_to_all | solution.py:51
  237.5 0.8 fusion.8
  238.3 41.1 %all_gather.10 = bf16[1024,256]{1,0:T(8,128)(2,1)S(1)} all-gather(bf16[64,256]{1,0:T(8,128)(2,1)S(1)} %get-tuple-element.14), channel_id=1, replica_groups=mesh['fs'=4,'rep'=4,'tp'=2] {'fs','rep'}, dimensions={0}, use_global_device_ids=true | all-gather | bytes 557056 | tf_op jit(solution)/shard_map/all_gather | solution.py:112
  279.4 0.8 copy.23
  280.2 0.6 copy-done.1
  280.8 1.0 copy.24
  (25 shorter events, 0.2 us)
Async XLA Ops:
  7.2 1.0 copy-start
  7.2 2.2 copy-start.3
  7.2 131.7 %reduce-scatter.2.cloned.1.call-start = ((), (), s32[]{:S(2)}) async-start(), calls=%async_computation.2 | async-start | bytes 417792 | tf_op jit(solution)/shard_map/reduce_scatter | solution.py:69
  8.1 1.5 copy-start.4
  9.3 1.0 copy-start.2
  10.3 0.8 copy-start.5
  12.5 126.4 %copy-start.9 = (f32[8,512]{1,0:T(8,128)S(1)}, f32[8,512]{1,0:T(8,128)}, u32[]{:S(2)}) copy-start(f32[8,512]{1,0:T(8,128)} %param.20) | copy-start | bytes 49156
  12.6 126.4 %copy-start.8 = (f32[8,512]{1,0:T(8,128)S(1)}, f32[8,512]{1,0:T(8,128)}, u32[]{:S(2)}) copy-start(f32[8,512]{1,0:T(8,128)} %param.21) | copy-start | bytes 49156
  12.6 266.8 %all-gather.2.cloned.1.call-start = ((), (), s32[]{:S(2)}) async-start(), calls=%async_computation.3 | async-start | bytes 1114112 | tf_op jit(solution)/shard_map/all_gather | solution.py:113
  12.6 128.2 %copy-start.10 = (f32[8,256]{1,0:T(8,128)S(1)}, f32[8,256]{1,0:T(8,128)}, u32[]{:S(2)}) copy-start(f32[8,256]{1,0:T(8,128)} %param.19) | copy-start | bytes 24580
  12.6 128.2 %copy-start.11 = (f32[8,256]{1,0:T(8,128)S(1)}, f32[8,256]{1,0:T(8,128)}, u32[]{:S(2)}) copy-start(f32[8,256]{1,0:T(8,128)} %param.18) | copy-start | bytes 24580
  183.9 40.4 %copy-start.6 = (f32[64,512]{1,0:T(8,128)S(1)}, f32[64,512]{1,0:T(8,128)}, u32[]{:S(2)}) copy-start(f32[64,512]{1,0:T(8,128)} %param.17) | copy-start | bytes 393220
  225.9 11.6 %copy-start.7 = (f32[64,256]{1,0:T(8,128)S(1)}, f32[64,256]{1,0:T(8,128)}, u32[]{:S(2)}) copy-start(f32[64,256]{1,0:T(8,128)} %param.16) | copy-start | bytes 196612
  225.9 11.6 %all-to-all-start = ((f32[16,8,256]{2,1,0:T(8,128)}), f32[16,8,256]{2,1,0:T(8,128)S(1)}, u32[]{:S(2)}, u32[]{:S(2)}) async-start(f32[16,8,256]{2,1,0:T(8,128)} %stack.2), calls=%async_computation.1 | async-start | bytes 262144 | tf_op jit(solution)/shard_map/all_to_all | solution.py:51
  279.4 1.4 copy-start.1
Sparse Core Ops, SparseCore 0:
  13.2 125.6 reduce-scatter.1
  225.3 52.6 all-gather.1

commit v2 on v0

--- a/solution.py
+++ b/solution.py
@@ -77,8 +77,14 @@
         lax.all_gather(query_dir, ("fs", "rep"), axis=0, tiled=True),
         lax.all_gather(value_dir, ("fs", "rep"), axis=0, tiled=True),
     )
-    query_squares, value_squares = lax.psum(
-        (jnp.sum(query_dir * query_dir), jnp.sum(value_dir * value_dir)), ("fs", "rep", "tp")
+
+    def produce_the_bench(my_data, axis_name, named_axis):
+        for u in (axis_name, named_axis):
+            my_data = lax.psum(my_data, u)
+        return my_data
+
+    query_squares, value_squares = produce_the_bench(
+        (jnp.sum(query_dir * query_dir), jnp.sum(value_dir * value_dir)), ("rep", "tp"), "fs"
     )
     tp_count = lax.axis_size("tp")
     query_update, query_weight_new, query_half = finish(

time: 314 us -> 294 us (0.936)
  blocking collectives: 159 us -> 138 us
    psum x1 -> x2, blocking collectives: 40.4 us -> 23.8 us  [produce_the_bench(): my_data = lax.psum(my_data, u)]
    all_gather x1, blocking collectives: 40.3 us -> 37 us  [body(): lax.all_gather(value_dir, ('fs', 'rep'), axis=0, tiled=True)]
where the time goes in v2:
time: 294 us; the launch traced here: 293 us
  blocking collectives  138 us (47%)
  waiting for transfers between devices  126 us (43%)
  between operations  15.6 us (5%)
  local copies, waits for them, and re-layouts  4.65 us (2%)
  other arithmetic  4.61 us (2%)
  matrix products  4.03 us (1%)
    reduce_scatter x1, waiting for transfers between devices, body(): lax.psum_scatter(jnp.concatenate([parts_product(query_high, query_low, qu...  126 us
    all_gather x1, blocking collectives, body(): lax.all_gather(query_half, ('fs', 'rep'), axis=0, tiled=True)  38.8 us
    all_gather x1, blocking collectives, body(): lax.all_gather(query_dir, ('fs', 'rep'), axis=0, tiled=True)  38.4 us
    all_gather x1, blocking collectives, body(): lax.all_gather(value_dir, ('fs', 'rep'), axis=0, tiled=True)  37 us
    psum x2, blocking collectives, produce_the_bench(): my_data = lax.psum(my_data, u)  23.8 us
  transfers between devices with their start and end apart: 2, of which 1 were waited for; matrix products, arithmetic and copies ran while one was open for 0% of the time, Pallas kernels for 0%

profile of v2, /device:TPU:0, one launch (start us, length us, event | category | flops | bytes accessed | tf_op | source)
XLA Modules:
  0.0 293.2 jit_solution(6767087489298853209)
XLA Ops:
  7.2 0.9 copy-done
  8.1 1.2 fusion.10
  9.4 0.2 fusion.13
  9.6 0.7 copy-done.2
  10.3 0.2 fusion.11
  10.5 0.6 copy-done.5
  11.1 0.2 fusion.12
  11.3 0.2 convolution_add_fusion
  11.6 0.2 convolution_add_fusion.1
  11.8 0.8 pad_maximum_fusion
  12.6 0.0 all-gather.2.cloned.1.call-start
  12.7 126.3 %reduce-scatter.2.cloned.1.call-done = f32[8,768]{1,0:T(8,128)} async-done(((f32[128,768]{1,0:T(8,128)}), f32[8,768]{1,0:T(8,128)}) %reduce-scatter.2.cloned.1.call-update) | async-done | bytes 24592 | tf_op jit(solution)/shard_map/reduce_scatter | solution.py:56
  138.9 1.9 multiply_reduce_fusion
  140.9 1.9 multiply_reduce_fusion.1
  142.8 12.5 %all-reduce = (f32[]{:T(128)}, f32[]{:T(128)}) all-reduce(f32[]{:T(128)} %get-tuple-element.22, f32[]{:T(128)} %get-tuple-element.18), channel_id=1, replica_groups=mesh['fs'=4,'rep'=4,'tp'=2] {'rep','tp'}, use_global_device_ids=true, to_apply=%region_2.0 | all-reduce | flops 2 | bytes 16 | tf_op jit(solution)/shard_map/psum | solution.py:83
  155.2 11.3 %all-reduce.1 = (f32[]{:T(128)}, f32[]{:T(128)}) all-reduce(f32[]{:T(128)} %get-tuple-element.10, f32[]{:T(128)} %get-tuple-element.11), channel_id=1, replica_groups=mesh['fs'=4,'rep'=4,'tp'=2] {'fs'}, use_global_device_ids=true, to_apply=%region_3.0 | all-reduce | flops 2 | bytes 16 | tf_op jit(solution)/shard_map/psum | solution.py:83
  167.3 37.0 %all_gather.13 = f32[128,512]{1,0:T(8,128)S(1)} all-gather(f32[8,512]{1,0:T(8,128)S(1)} %get-tuple-element.19), channel_id=1, replica_groups=mesh['fs'=4,'rep'=4,'tp'=2] {'fs','rep'}, dimensions={0}, use_global_device_ids=true | all-gather | bytes 278528 | tf_op jit(solution)/shard_map/all_gather | solution.py:78
  204.3 1.0 fusion.6
  206.0 38.4 %all_gather.12 = f32[128,256]{1,0:T(8,128)S(1)} all-gather(f32[8,256]{1,0:T(8,128)S(1)} %get-tuple-element.23), channel_id=1, replica_groups=mesh['fs'=4,'rep'=4,'tp'=2] {'fs','rep'}, dimensions={0}, use_global_device_ids=true | all-gather | bytes 139264 | tf_op jit(solution)/shard_map/all_gather | solution.py:77
  244.4 0.8 fusion.7
  245.2 38.8 %all_gather.14 = bf16[1024,256]{1,0:T(8,128)(2,1)S(1)} all-gather(bf16[64,256]{1,0:T(8,128)(2,1)S(1)} %get-tuple-element.16), channel_id=1, replica_groups=mesh['fs'=4,'rep'=4,'tp'=2] {'fs','rep'}, dimensions={0}, use_global_device_ids=true | all-gather | bytes 557056 | tf_op jit(solution)/shard_map/all_gather | solution.py:105
  284.0 0.8 copy.23
  284.8 0.6 copy-done.1
  285.4 1.0 copy.24
  (24 shorter events, 0.1 us)
Async XLA Ops:
  7.2 1.0 copy-start
  7.2 2.2 copy-start.3
  7.2 131.7 %reduce-scatter.2.cloned.1.call-start = ((), (), s32[]{:S(2)}) async-start(), calls=%async_computation.1 | async-start | bytes 417792 | tf_op jit(solution)/shard_map/reduce_scatter | solution.py:56
  8.1 1.5 copy-start.4
  9.3 1.0 copy-start.2
  10.3 0.8 copy-start.5
  12.5 126.4 %copy-start.9 = (f32[8,512]{1,0:T(8,128)S(1)}, f32[8,512]{1,0:T(8,128)}, u32[]{:S(2)}) copy-start(f32[8,512]{1,0:T(8,128)} %param.20) | copy-start | bytes 49156
  12.6 126.4 %copy-start.8 = (f32[8,512]{1,0:T(8,128)S(1)}, f32[8,512]{1,0:T(8,128)}, u32[]{:S(2)}) copy-start(f32[8,512]{1,0:T(8,128)} %param.21) | copy-start | bytes 49156
  12.6 271.4 %all-gather.2.cloned.1.call-start = ((), (), s32[]{:S(2)}) async-start(), calls=%async_computation.2 | async-start | bytes 1114112 | tf_op jit(solution)/shard_map/all_gather | solution.py:106
  12.6 128.2 %copy-start.10 = (f32[8,256]{1,0:T(8,128)S(1)}, f32[8,256]{1,0:T(8,128)}, u32[]{:S(2)}) copy-start(f32[8,256]{1,0:T(8,128)} %param.19) | copy-start | bytes 24580
  12.6 128.2 %copy-start.11 = (f32[8,256]{1,0:T(8,128)S(1)}, f32[8,256]{1,0:T(8,128)}, u32[]{:S(2)}) copy-start(f32[8,256]{1,0:T(8,128)} %param.18) | copy-start | bytes 24580
  167.2 37.0 %copy-start.6 = (f32[64,512]{1,0:T(8,128)S(1)}, f32[64,512]{1,0:T(8,128)}, u32[]{:S(2)}) copy-start(f32[64,512]{1,0:T(8,128)} %param.17) | copy-start | bytes 393220
  206.0 38.4 %copy-start.7 = (f32[64,256]{1,0:T(8,128)S(1)}, f32[64,256]{1,0:T(8,128)}, u32[]{:S(2)}) copy-start(f32[64,256]{1,0:T(8,128)} %param.16) | copy-start | bytes 196612
  284.0 1.4 copy-start.1
Sparse Core Ops, SparseCore 0:
  13.2 125.6 reduce-scatter.1
  205.4 54.4 all-gather.1
